TPU v7x, 512 devices: a 8x2x16 block of a 8x8x16 slice. The times are simulated.
512 devices in a mesh: grp: 2 (over y), sp: 16 (over z), tp: 16 (over x, core).
Axes of the slice: x: 8, y: 2, z: 16, core: 2. Of those that a mesh axis runs over, the one named last changes fastest.
The devices are a block of a 8x8x16 slice.
Arguments:
- latent: bfloat16 [16384, 4096], P(('grp', 'sp'), 'tp'), parts along dimension 0, may hold values from -42 to 42
- context: bfloat16 [2048, 4096], P(('grp', 'sp'), 'tp'), parts along dimension 0, may hold values from -42 to 42
- conditions: float32 [4, 4096], P('grp', 'sp'), parts along dimension 0, may hold values from -6 to 6
- mod_weight: bfloat16 [4096, 3, 4096], P('sp', None, 'tp'), may hold values from -0.09375 to 0.09375
- norm_gain: float32 [4096], P('tp'), may hold values from 0.1 to 1.9
- w_query: bfloat16 [4096, 2048], P(None, 'tp'), may hold values from -0.09375 to 0.09375
- w_key: bfloat16 [4096, 2048], P(None, 'tp'), may hold values from -0.09375 to 0.09375
- w_value: bfloat16 [4096, 2048], P(None, 'tp'), may hold values from -0.09375 to 0.09375
- query_gain: float32 [64], replicated, may hold values from 1 to 14
- key_gain: float32 [64], replicated, may hold values from 1 to 14
- lambdas: float32 [16], P('tp'), may hold values from 0.3 to 0.8
- out_gain: float32 [128], replicated, may hold values from 0.1 to 1.9
- w_out: bfloat16 [2048, 4096], P(None, 'tp'), may hold values from -0.125 to 0.125
Outputs:
- updated: bfloat16 [16384, 4096], P(('grp', 'sp'), 'tp'), parts along dimension 0
There are 2 independent parts, one for each index of `grp`. A program takes and returns all parts, laid end to end along the dimension named above; an argument that names none is the same for every part. Nothing has to cross between parts.
All inputs are finite; a program needn't handle non-finite values.
Results may differ from a plain program's by a relative error of at most 0.0076.
Values may be sent and summed in bfloat16 or wider, within the bound.
A program may use at most 64 MiB of HBM per device.

v0:
```python
import math
import jax
import jax.numpy as jnp
from jax import lax
from jax.sharding import PartitionSpec as P

DK = 64
DV = 128
GRID_W = 64
epsilon = 1e-06


def sent_to_all(value, axis):
    size = lax.axis_size(axis)
    return lax.all_to_all(
        jnp.broadcast_to(value[None], (size, *value.shape)), axis, 0, 0, tiled=True
    )


def of_everyone(value, axis):
    everything = sent_to_all(value, axis)
    return jnp.sum(everything, axis=0)


def in_one_piece(arrays, axis, dim, along):
    both = jnp.concatenate(arrays, axis=along)
    whole, at, gathered = (lax.all_gather(both, axis, axis=dim, tiled=True), 0, [])
    for a in arrays:
        gathered.append(lax.slice_in_dim(whole, at, at + a.shape[along], axis=along))
        at += a.shape[along]
    return tuple(gathered)


def turn_half(halves, angles):
    quarter = halves.shape[-1] // 2
    cosine = jnp.cos(angles)[:, None, None, :]
    sine_part = jnp.sin(angles)[:, None, None, :]
    first_part = halves[..., :quarter]
    second = halves[..., quarter:]
    return jnp.concatenate(
        [first_part * cosine - second * sine_part, first_part * sine_part + second * cosine],
        axis=-1,
    )


def rotate(features, positions):
    half_width = features.shape[-1] // 2
    quarter = half_width // 2
    inverse = 10000.0 ** (-2.0 * jnp.arange(quarter, dtype=jnp.float32) / half_width)
    grid_row = (positions // GRID_W).astype(jnp.float32)
    grid_column = (positions % GRID_W).astype(jnp.float32)
    return jnp.concatenate(
        [
            turn_half(features[..., :half_width], grid_row[:, None] * inverse),
            turn_half(features[..., half_width:], grid_column[:, None] * inverse),
        ],
        axis=-1,
    )


def head_norm(features, gain_row):
    return (
        features
        * lax.rsqrt(jnp.mean(features * features, axis=-1, keepdims=True) + epsilon)
        * gain_row
    )


def modulate(rows_in, gain_row, shift_row, scale_row):
    floats = rows_in.astype(jnp.float32)
    factor = lax.rsqrt(jnp.mean(floats * floats, axis=1, keepdims=True) + epsilon)
    return (floats * factor * gain_row * (1.0 + scale_row) + shift_row).astype(jnp.bfloat16)


def local(
    latent,
    context,
    conditions,
    mod_weight,
    norm_gain,
    w_query,
    w_key,
    w_value,
    query_gain,
    key_gain,
    lambdas,
    out_gain,
    w_out,
):
    tok_rows = latent.shape[0]
    ctx_rows = context.shape[0]
    columns = latent.shape[1]
    heads_here = lambdas.shape[0]
    in_rows = mod_weight.shape[0]
    activated = jax.nn.silu(conditions).astype(jnp.bfloat16)
    partial_mod = jnp.dot(
        activated, mod_weight.reshape(in_rows, 3 * columns), preferred_element_type=jnp.float32
    ).reshape(2, 3, columns)
    modulation = of_everyone(partial_mod, "sp")
    lat_floats = latent.astype(jnp.float32)
    full_gain, full_pairs = (
        lax.all_gather(norm_gain, "tp", axis=0, tiled=True),
        lax.all_gather(modulation[:, :2], "tp", axis=2, tiled=True),
    )
    whole_lat, whole_ctx = in_one_piece((latent, context), "tp", 1, 0)
    hidden = modulate(whole_lat, full_gain, full_pairs[0, 0], full_pairs[0, 1])
    hidden_ctx = modulate(whole_ctx, full_gain, full_pairs[1, 0], full_pairs[1, 1])
    query_raw = jnp.dot(hidden, w_query, preferred_element_type=jnp.float32)
    key_raw = jnp.dot(hidden, w_key, preferred_element_type=jnp.float32)
    value_raw = jnp.dot(hidden, w_value, preferred_element_type=jnp.float32)
    ctx_key_raw = jnp.dot(hidden_ctx, w_key, preferred_element_type=jnp.float32)
    ctx_value_raw = jnp.dot(hidden_ctx, w_value, preferred_element_type=jnp.float32)
    positions = lax.axis_index("sp") * tok_rows + jnp.arange(tok_rows, dtype=jnp.int32)
    queries = rotate(
        head_norm(query_raw.reshape(tok_rows, heads_here, 2, DK), query_gain), positions
    ).astype(jnp.bfloat16)
    lat_keys = (
        rotate(head_norm(key_raw.reshape(tok_rows, heads_here, 2, DK), key_gain), positions)
        .astype(jnp.bfloat16)
        .reshape(tok_rows, heads_here * 2 * DK)
    )
    lat_values = value_raw.astype(jnp.bfloat16)
    ctx_keys = (
        head_norm(ctx_key_raw.reshape(ctx_rows, heads_here, 2, DK), key_gain)
        .astype(jnp.bfloat16)
        .reshape(ctx_rows, heads_here * 2 * DK)
    )
    ctx_values = ctx_value_raw.astype(jnp.bfloat16)
    scaling = DK ** (-0.5)

    def absorb(carried, key_rows, value_rows):
        key_count = key_rows.shape[0]
        key_block = key_rows.reshape(key_count, heads_here, 2, DK)
        value_block = value_rows.reshape(key_count, heads_here, DV)
        running_max, totals, weighted = carried
        scores = (
            jnp.einsum("qhmd,khmd->qhmk", queries, key_block, preferred_element_type=jnp.float32)
            * scaling
        )
        new_max = jnp.maximum(running_max, jnp.max(scores, axis=-1))
        rescale = jnp.exp(running_max - new_max)
        exponent = jnp.exp(scores - new_max[..., None])
        totals = totals * rescale + jnp.sum(exponent, axis=-1)
        weighted = weighted * rescale[..., None] + jnp.einsum(
            "qhmk,khv->qhmv",
            exponent.astype(jnp.bfloat16),
            value_block,
            preferred_element_type=jnp.float32,
        )
        return (new_max, totals, weighted)

    def absorb_rows(carried, key_rows, value_rows):
        key_count = key_rows.shape[0]
        block_rows = math.gcd(key_count, 512)

        def visit_block(block_index, partial_value):
            first_row = block_index * block_rows
            return absorb(
                partial_value,
                lax.dynamic_slice_in_dim(key_rows, first_row, block_rows, 0),
                lax.dynamic_slice_in_dim(value_rows, first_row, block_rows, 0),
            )

        return lax.fori_loop(0, key_count // block_rows, visit_block, carried)

    initial_state = (
        jnp.full((tok_rows, heads_here, 2), -1e30, jnp.float32),
        jnp.zeros((tok_rows, heads_here, 2), jnp.float32),
        jnp.zeros((tok_rows, heads_here, 2, DV), jnp.float32),
    )
    every_ctx_keys, every_ctx_values = in_one_piece((ctx_keys, ctx_values), "sp", 0, 1)
    carried = absorb_rows(initial_state, every_ctx_keys, every_ctx_values)
    pieces = in_one_piece((lat_keys, lat_values), "sp", 0, 1)
    carried = absorb_rows(carried, pieces[0], pieces[1])
    running_max, totals, weighted = carried
    attended = (
        weighted[:, :, 0] / totals[:, :, 0, None]
        - lambdas[None, :, None] * weighted[:, :, 1] / totals[:, :, 1, None]
    )
    head_out = head_norm(attended, out_gain).astype(jnp.bfloat16).reshape(tok_rows, heads_here * DV)
    mixed_rows = jnp.dot(
        lax.all_gather(head_out, "tp", axis=1, tiled=True),
        w_out,
        preferred_element_type=jnp.float32,
    )
    return (lat_floats + modulation[0, 2] * mixed_rows).astype(jnp.bfloat16)


def solution(mesh):
    in_specs = (
        P(("grp", "sp"), "tp"),
        P(("grp", "sp"), "tp"),
        P("grp", "sp"),
        P("sp", None, "tp"),
        P("tp"),
        P(None, "tp"),
        P(None, "tp"),
        P(None, "tp"),
        P(),
        P(),
        P("tp"),
        P(),
        P(None, "tp"),
    )
    out_specs = P(("grp", "sp"), "tp")
    return jax.shard_map(local, mesh=mesh, in_specs=in_specs, out_specs=out_specs, check_vma=False)
```

profile of v0, /device:TPU:65, one launch (start us, length us, event | category | flops | bytes accessed | tf_op | source)
XLA Modules:
  0.0 304.0 jit_solution(5467779890000573192)
XLA Ops:
  6.6 1.8 pad_maximum_fusion
  11.2 44.2 %all-to-all-start = ((f32[16,2,3,256]{3,1,2,0:T(2,128)}), f32[16,2,3,256]{3,1,2,0:T(2,128)S(1)}, u32[]{:S(2)}, u32[]{:S(2)}) async-start(f32[16,2,3,256]{3,1,2,0:T(2,128)} %broadcast_in_dim.16), calls=%async_computation | async-start | bytes 196608 | tf_op jit(solution)/shard_map/all_to_all | solution.py:15
  55.5 18.9 %all-gather = f32[16,1,256]{2,1,0:T(1,128)S(1)} all-gather(f32[1,1,256]{2,1,0:T(1,128)S(1)} %bitcast.220), channel_id=1, replica_groups=mesh['grp'=2,'sp'=16,'tp'=16] {'tp'}, dimensions={0}, use_global_device_ids=true | all-gather | bytes 17408 | tf_op jit(solution)/shard_map/all_gather | solution.py:102
  74.8 15.3 %all_gather.20 = f32[2,2,4096]{2,0,1:T(2,128)S(1)} all-gather(f32[2,2,256]{2,0,1:T(2,128)S(1)} %slice.110), channel_id=1, replica_groups=mesh['grp'=2,'sp'=16,'tp'=16] {'tp'}, dimensions={2}, use_global_device_ids=true | all-gather | bytes 69632 | tf_op jit(solution)/shard_map/all_gather | solution.py:103
  90.2 13.1 %all-gather.5.cloned.1.call-done = bf16[576,4096]{1,0:T(8,128)(2,1)} async-done(((bf16[576,256]{1,0:T(8,128)(2,1)}), bf16[576,4096]{1,0:T(8,128)(2,1)}) %all-gather.5.cloned.1.call-update) | async-done | bytes 4718608 | tf_op jit(solution)/shard_map/all_gather | solution.py:27
  103.3 3.1 %fusion.30 = f32[512]{0:T(512)S(1)} fusion(bf16[576,4096]{1,0:T(8,128)(2,1)} %all-gather.5.cloned.1.call-done), kind=kLoop, calls=%fused_computation.47 | loop fusion | flops 6290944 | bytes 4196352 | tf_op jit(solution)/shard_map/reduce_sum | solution.py:71
  106.4 3.4 %fusion.34 = bf16[512,4096]{1,0:T(8,128)(2,1)S(1)} fusion(f32[4096]{0:T(1024)S(1)} %bitcast.211, f32[4096]{0:T(1024)S(1)} %bitcast.210, f32[4096]{0:T(1024)S(1)} %bitcast.207, f32[512]{0:T(512)S(1)} %add_rsqrt_fusion.4, bf16[576,4096]{1,0:T(8,128)(2,1)} %all-gather.5.cloned.1.call-done), kind=kLoop, calls=%fused_computation.51 | loop fusion | flops 12582912 | bytes 8439808 | tf_op jit(solution)/shard_map/convert_element_type | solution.py:72
  109.8 1.5 convolution_convert_fusion
  116.5 1.8 fusion.66
  118.8 1.5 convolution_convert_fusion.1
  120.4 3.7 %fusion.67 = f32[512,128]{0,1:T(8,128)S(1)} fusion(bf16[512,4096]{1,0:T(8,128)(2,1)} %copy-done.1, bf16[4096,128]{1,0:T(8,128)(2,1)S(1)} %copy-done.4), kind=kOutput, calls=%fused_computation.130 | convolution fusion | flops 536870912 | bytes 5505024 | tf_op jit(solution)/shard_map/dot_general | solution.py:108
  124.3 29.9 %all_gather.21 = bf16[1024,256]{1,0:T(8,128)(2,1)S(1)} all-gather(bf16[64,256]{1,0:T(8,128)(2,1)S(1)} %pad_maximum_fusion.4), channel_id=1, replica_groups=mesh['grp'=2,'sp'=16,'tp'=16] {'sp'}, dimensions={0}, use_global_device_ids=true | all-gather | bytes 557056 | tf_op jit(solution)/shard_map/all_gather | solution.py:27
  154.2 3.5 %while.36 = (s32[]{:T(128)}, f32[512,1,2]{0,2,1:T(2,128)S(1)}, f32[512,1,2]{0,2,1:T(2,128)S(1)}, f32[512,1,2,128]{0,3,2,1:T(8,128)S(1)}, bf16[1024,128]{1,0:T(8,...) while((s32[]{:T(128)}, f32[512,1,2]{0,2,1:T(2,128)S(1)}, ...), condition=%wide.region_8.9_spmd.clone, body=%wide.region_5.8_spmd.clone.sunk | while | flops 205920256 | bytes 8323255 | solution.py:164
  157.7 28.5 %all-gather.7.cloned.1.call-done = bf16[8192,256]{0,1:T(8,128)(2,1)} async-done(((bf16[512,256]{0,1:T(8,128)(2,1)}), bf16[8192,256]{0,1:T(8,128)(2,1)}) %all-gather.7.cloned.1.call-update) | async-done | bytes 4194320 | tf_op jit(solution)/shard_map/all_gather | solution.py:27
  186.2 4.6 %fusion.63 = (bf16[8192,128]{0,1:T(8,128)(2,1)}, bf16[8192,128]{0,1:T(8,128)(2,1)}) fusion(bf16[8192,256]{0,1:T(8,128)(2,1)} %all-gather.7.cloned.1.call-done), kind=kLoop, calls=%fused_computation.126 | loop fusion | bytes 8388608 | tf_op jit(solution)/shard_map/slice | solution.py:29
  190.8 54.4 %while.35 = (s32[]{:T(128)}, f32[512,1,2]{0,2,1:T(2,128)S(1)}, f32[512,1,2]{0,2,1:T(2,128)S(1)}, f32[512,1,2,128]{0,3,2,1:T(8,128)S(1)}, bf16[8192,128]{0,1:T(8,...) while((s32[]{:T(128)}, f32[512,1,2]{0,2,1:T(2,128)S(1)}, ...), condition=%wide.region_13.14_spmd, body=%wide.region_10.13_spmd.sunk | while | flops 205786112 | bytes 8061091 | solution.py:164
  192.7 1.5 fusion.98
  196.1 1.5 fusion.98
  209.7 1.5 fusion.98
  216.5 1.5 fusion.98
  223.2 1.5 fusion.98
  230.0 1.5 fusion.98
  246.1 48.3 %all-gather.9.cloned.1.call-done = bf16[512,2048]{0,1:T(8,128)(2,1)} async-done(((bf16[512,128]{0,1:T(8,128)(2,1)}), bf16[512,2048]{0,1:T(8,128)(2,1)}) %all-gather.9.cloned.1.call-update) | async-done | bytes 2097168 | tf_op jit(solution)/shard_map/all_gather | solution.py:182
  294.4 3.1 %fusion.36 = bf16[512,256]{1,0:T(8,128)(2,1)} fusion(bf16[512,2048]{0,1:T(8,128)(2,1)} %all-gather.9.cloned.1.call-done, bf16[2048,256]{1,0:T(8,128)(2,1)S(1)} %copy-done, bf16[512,256]{1,0:T(8,128)(2,1)S(1)} %copy-done.5, f32[256]{0:T(256)S(1)} %bitcast.221), kind=kOutput, calls=%fused_computation.56 | convolution fusion | flops 537395200 | bytes 3671040 | tf_op jit(solution)/shard_map/dot_general | solution.py:181
  (191 shorter events, 57.0 us)
Async XLA Ops:
  6.5 287.9 %copy-start = (bf16[2048,256]{1,0:T(8,128)(2,1)S(1)}, bf16[2048,256]{1,0:T(8,128)(2,1)}, u32[]{:S(2)}) copy-start(bf16[2048,256]{1,0:T(8,128)(2,1)} %param.29) | copy-start | bytes 3145732
  6.6 49.0 %copy-start.6 = (f32[256]{0:T(256)S(1)}, f32[256]{0:T(256)}, u32[]{:S(2)}) copy-start(f32[256]{0:T(256)} %param.21) | copy-start | bytes 3076
  6.6 96.7 %all-gather.5.cloned.1.call-start = ((), (), s32[]{:S(2)}) async-start(), calls=%async_computation.1 | async-start | bytes 5013504 | tf_op jit(solution)/shard_map/all_gather | solution.py:27
  11.2 63.6 %all-to-all-start = ((f32[16,2,3,256]{3,1,2,0:T(2,128)}), f32[16,2,3,256]{3,1,2,0:T(2,128)S(1)}, u32[]{:S(2)}, u32[]{:S(2)}) async-start(f32[16,2,3,256]{3,1,2,0:T(2,128)} %broadcast_in_dim.16), calls=%async_computation | async-start | bytes 196608 | tf_op jit(solution)/shard_map/all_to_all | solution.py:15
  55.4 130.8 %all-gather.7.cloned.1.call-start = ((), (), s32[]{:S(2)}) async-start(), calls=%async_computation.2 | async-start | bytes 4456448 | tf_op jit(solution)/shard_map/all_gather | solution.py:27
  106.4 3.4 %copy-start.2 = (bf16[4096,128]{1,0:T(8,128)(2,1)S(1)}, bf16[4096,128]{1,0:T(8,128)(2,1)}, u32[]{:S(2)}) copy-start(bf16[4096,128]{1,0:T(8,128)(2,1)} %param.24) | copy-start | bytes 3145732
  109.8 2.0 copy-start.1
  109.8 2.0 copy-start.3
  111.8 1.6 copy-start.7
  114.4 180.1 %all-gather.9.cloned.1.call-start = ((), (), s32[]{:S(2)}) async-start(), calls=%async_computation.3 | async-start | bytes 2228224 | tf_op jit(solution)/shard_map/all_gather | solution.py:182
  118.8 1.6 copy-start.4
  120.4 3.8 %copy-start.8 = (f32[64]{0:T(128)S(1)}, f32[64]{0:T(128)}, u32[]{:S(2)}) copy-start(f32[64]{0:T(128)} %param.25) | copy-start | bytes 772
  190.8 54.5 %copy-start.9 = (f32[128]{0:T(128)S(1)}, f32[128]{0:T(128)}, u32[]{:S(2)}) copy-start(f32[128]{0:T(128)} %param.28) | copy-start | bytes 1540
  190.8 103.6 %copy-start.5 = (bf16[512,256]{1,0:T(8,128)(2,1)S(1)}, bf16[512,256]{1,0:T(8,128)(2,1)}, u32[]{:S(2)}) copy-start(bf16[512,256]{1,0:T(8,128)(2,1)} %param.17) | copy-start | bytes 786436
Sparse Core Ops, SparseCore 0:
  9.4 93.8 all-gather.4
  114.5 71.6 all-gather.6
  246.3 48.1 all-gather.8
where the time goes:
time: 305 us; the launch traced here: 304 us
  waiting for transfers between devices  90.1 us (30%)
  blocking collectives  64.1 us (21%)
  matrix products  48.7 us (16%)
  starting transfers between devices  44.4 us (15%)
  local copies, waits for them, and re-layouts  22.5 us (7%)
  other arithmetic  19.2 us (6%)
  between operations  14.1 us (5%)
    all_gather x1, waiting for transfers between devices, local(): lax.all_gather(head_out, 'tp', axis=1, tiled=True)  48.3 us
    all_to_all x1, starting transfers between devices, sent_to_all(): lax.all_to_all(jnp.broadcast_to(value[None], (size, *value.shape)), axis,...  44.2 us
    all_gather x2, waiting for transfers between devices, in_one_piece(): lax.all_gather(both, axis, axis=dim, tiled=True)  41.6 us
    all_gather x1, blocking collectives, in_one_piece(): lax.all_gather(both, axis, axis=dim, tiled=True)  29.9 us
    dot_general x18, matrix products, absorb(): jnp.einsum('qhmk,khv->qhmv', exponent.astype(jnp.bfloat16), value_block,...  25.7 us
    all_gather x1, blocking collectives, local(): lax.all_gather(norm_gain, 'tp', axis=0, tiled=True)  18.9 us
    all_gather x1, blocking collectives, local(): lax.all_gather(modulation[:, :2], 'tp', axis=2, tiled=True)  15.3 us
    dynamic_slice x20, local copies, waits for them, and re-layouts, visit_block(): lax.dynamic_slice_in_dim(key_rows, first_row, block_rows, 0)  15 us
  transfers between devices with their start and end apart: 4, of which 3 were waited for; matrix products, arithmetic and copies ran while one was open for 5% of the time, Pallas kernels for 0%

commit v1 on v0

--- a/solution.py
+++ b/solution.py
@@ -100,7 +100,9 @@
     lat_floats = latent.astype(jnp.float32)
     full_gain, full_pairs = (
         lax.all_gather(norm_gain, "tp", axis=0, tiled=True),
-        lax.all_gather(modulation[:, :2], "tp", axis=2, tiled=True),
+        jnp.concatenate(
+            lax.all_to_all(jnp.stack([modulation[:, :2]] * lax.axis_size("tp")), "tp", 0, 0), axis=2
+        ),
     )
     whole_lat, whole_ctx = in_one_piece((latent, context), "tp", 1, 0)
     hidden = modulate(whole_lat, full_gain, full_pairs[0, 0], full_pairs[0, 1])

time: 305 us -> 307 us (level)
  blocking collectives: 64.1 us -> 49.9 us
  waiting for transfers between devices: 90.1 us -> 101 us
  starting transfers between devices: 44.4 us -> 48.7 us
    all_gather x1 -> x0, blocking collectives: 15.3 us -> none  [local(): lax.all_gather(modulation[:, :2], 'tp', axis=2, tiled=True)]
    all_to_all x0 -> x1, waiting for transfers between devices: none -> 8.16 us  [local(): lax.all_to_all(jnp.stack([modulation[:, :2]] * lax.axis_size('tp')), 'tp'...]
    all_to_all x0 -> x1, starting transfers between devices: none -> 4.36 us  [local(): lax.all_to_all(jnp.stack([modulation[:, :2]] * lax.axis_size('tp')), 'tp'...]
  transfers between devices with their start and end apart: 4 -> 5, of which waited for: 3 -> 4; matrix products, arithmetic and copies ran while one was open for 5% -> 5% of each run, Pallas kernels for 0% -> 0%
where the time goes in v1:
time: 307 us; the launch traced here: 306 us
  waiting for transfers between devices  101 us (33%)
  blocking collectives  49.9 us (16%)
  starting transfers between devices  48.7 us (16%)
  matrix products  48.7 us (16%)
  local copies, waits for them, and re-layouts  23.1 us (8%)
  other arithmetic  19.2 us (6%)
  between operations  14.2 us (5%)
    all_gather x1, waiting for transfers between devices, local(): lax.all_gather(head_out, 'tp', axis=1, tiled=True)  48.9 us
    all_to_all x1, starting transfers between devices, sent_to_all(): lax.all_to_all(jnp.broadcast_to(value[None], (size, *value.shape)), axis,...  44.2 us
    all_gather x2, waiting for transfers between devices, in_one_piece(): lax.all_gather(both, axis, axis=dim, tiled=True)  44 us
    all_gather x1, blocking collectives, in_one_piece(): lax.all_gather(both, axis, axis=dim, tiled=True)  31 us
    dot_general x18, matrix products, absorb(): jnp.einsum('qhmk,khv->qhmv', exponent.astype(jnp.bfloat16), value_block,...  25.7 us
    all_gather x1, blocking collectives, local(): lax.all_gather(norm_gain, 'tp', axis=0, tiled=True)  18.9 us
    dynamic_slice x20, local copies, waits for them, and re-layouts, visit_block(): lax.dynamic_slice_in_dim(key_rows, first_row, block_rows, 0)  15 us
    dot_general x18, matrix products, absorb(): jnp.einsum('qhmd,khmd->qhmk', queries, key_block, preferred_element_type=...  9.01 us
  transfers between devices with their start and end apart: 5, of which 4 were waited for; matrix products, arithmetic and copies ran while one was open for 5% of the time, Pallas kernels for 0%

profile of v1, /device:TPU:65, one launch (start us, length us, event | category | flops | bytes accessed | tf_op | source)
XLA Modules:
  0.0 306.1 jit_solution(9176195008581425117)
XLA Ops:
  6.6 1.8 pad_maximum_fusion
  11.2 44.2 %all-to-all-start = ((f32[16,2,3,256]{3,1,2,0:T(2,128)}), f32[16,2,3,256]{3,1,2,0:T(2,128)S(1)}, u32[]{:S(2)}, u32[]{:S(2)}) async-start(f32[16,2,3,256]{3,1,2,0:T(2,128)} %broadcast_in_dim.16), calls=%async_computation | async-start | bytes 196608 | tf_op jit(solution)/shard_map/all_to_all | solution.py:15
  55.5 18.9 %all-gather = f32[16,1,256]{2,1,0:T(1,128)S(1)} all-gather(f32[1,1,256]{2,1,0:T(1,128)S(1)} %bitcast.225), channel_id=1, replica_groups=mesh['grp'=2,'sp'=16,'tp'=16] {'tp'}, dimensions={0}, use_global_device_ids=true | all-gather | bytes 17408 | tf_op jit(solution)/shard_map/all_gather | solution.py:102
  75.1 4.4 %all-to-all-start.1 = ((f32[16,2,2,256]{3,2,1,0:T(2,128)}), f32[16,2,2,256]{3,2,1,0:T(2,128)S(1)}, u32[]{:S(2)}, u32[]{:S(2)}) async-start(f32[16,2,2,256]{3,2,1,0:T(2,128)} %stack.2), calls=%async_computation.1 | async-start | bytes 131072 | tf_op jit(solution)/shard_map/all_to_all | solution.py:104
  79.8 8.2 %all-to-all-done.1 = f32[16,2,2,256]{3,2,1,0:T(2,128)S(1)} async-done(((f32[16,2,2,256]{3,2,1,0:T(2,128)}), f32[16,2,2,256]{3,2,1,0:T(2,128)S(1)}, u32[]{:S(2)}, u32[]{:S(2)}) %all-to-all-start.1) | async-done | bytes 65568 | tf_op jit(solution)/shard_map/all_to_all | solution.py:104
  88.1 16.2 %all-gather.5.cloned.1.call-done = bf16[576,4096]{1,0:T(8,128)(2,1)} async-done(((bf16[576,256]{1,0:T(8,128)(2,1)}), bf16[576,4096]{1,0:T(8,128)(2,1)}) %all-gather.5.cloned.1.call-update) | async-done | bytes 4718608 | tf_op jit(solution)/shard_map/all_gather | solution.py:27
  104.2 3.1 %fusion.30 = f32[512]{0:T(512)S(1)} fusion(bf16[576,4096]{1,0:T(8,128)(2,1)} %all-gather.5.cloned.1.call-done), kind=kLoop, calls=%fused_computation.47 | loop fusion | flops 6290944 | bytes 4196352 | tf_op jit(solution)/shard_map/reduce_sum | solution.py:71
  107.3 3.4 %fusion.34 = bf16[512,4096]{1,0:T(8,128)(2,1)S(1)} fusion(f32[4096]{0:T(1024)S(1)} %bitcast.216, f32[4096]{0:T(1024)S(1)} %bitcast.215, f32[4096]{0:T(1024)S(1)} %bitcast.212, f32[512]{0:T(512)S(1)} %add_rsqrt_fusion.4, bf16[576,4096]{1,0:T(8,128)(2,1)} %all-gather.5.cloned.1.call-done), kind=kLoop, calls=%fused_computation.51 | loop fusion | flops 12582912 | bytes 8439808 | tf_op jit(solution)/shard_map/convert_element_type | solution.py:72
  117.4 1.8 fusion.66
  119.7 1.5 convolution_convert_fusion.1
  121.3 3.7 %fusion.67 = f32[512,128]{0,1:T(8,128)S(1)} fusion(bf16[512,4096]{1,0:T(8,128)(2,1)} %copy-done.1, bf16[4096,128]{1,0:T(8,128)(2,1)S(1)} %copy-done.4), kind=kOutput, calls=%fused_computation.130 | convolution fusion | flops 536870912 | bytes 5505024 | tf_op jit(solution)/shard_map/dot_general | solution.py:110
  125.2 31.0 %all_gather.17 = bf16[1024,256]{1,0:T(8,128)(2,1)S(1)} all-gather(bf16[64,256]{1,0:T(8,128)(2,1)S(1)} %pad_maximum_fusion.4), channel_id=1, replica_groups=mesh['grp'=2,'sp'=16,'tp'=16] {'sp'}, dimensions={0}, use_global_device_ids=true | all-gather | bytes 557056 | tf_op jit(solution)/shard_map/all_gather | solution.py:27
  156.3 3.5 %while.36 = (s32[]{:T(128)}, f32[512,1,2]{0,2,1:T(2,128)S(1)}, f32[512,1,2]{0,2,1:T(2,128)S(1)}, f32[512,1,2,128]{0,3,2,1:T(8,128)S(1)}, bf16[1024,128]{1,0:T(8,...) while((s32[]{:T(128)}, f32[512,1,2]{0,2,1:T(2,128)S(1)}, ...), condition=%wide.region_8.9_spmd.clone, body=%wide.region_5.8_spmd.clone.sunk | while | flops 205920256 | bytes 8323255 | solution.py:166
  159.8 27.9 %all-gather.7.cloned.1.call-done = bf16[8192,256]{0,1:T(8,128)(2,1)} async-done(((bf16[512,256]{0,1:T(8,128)(2,1)}), bf16[8192,256]{0,1:T(8,128)(2,1)}) %all-gather.7.cloned.1.call-update) | async-done | bytes 4194320 | tf_op jit(solution)/shard_map/all_gather | solution.py:27
  187.7 4.6 %fusion.63 = (bf16[8192,128]{0,1:T(8,128)(2,1)}, bf16[8192,128]{0,1:T(8,128)(2,1)}) fusion(bf16[8192,256]{0,1:T(8,128)(2,1)} %all-gather.7.cloned.1.call-done), kind=kLoop, calls=%fused_computation.126 | loop fusion | bytes 8388608 | tf_op jit(solution)/shard_map/slice | solution.py:29
  192.2 54.4 %while.35 = (s32[]{:T(128)}, f32[512,1,2]{0,2,1:T(2,128)S(1)}, f32[512,1,2]{0,2,1:T(2,128)S(1)}, f32[512,1,2,128]{0,3,2,1:T(8,128)S(1)}, bf16[8192,128]{0,1:T(8,...) while((s32[]{:T(128)}, f32[512,1,2]{0,2,1:T(2,128)S(1)}, ...), condition=%wide.region_13.14_spmd, body=%wide.region_10.13_spmd.sunk | while | flops 205786112 | bytes 8061091 | solution.py:166
  194.1 1.5 fusion.98
  197.5 1.5 fusion.98
  200.9 1.5 fusion.98
  204.3 1.5 fusion.98
  207.7 1.5 fusion.98
  211.1 1.5 fusion.98
  247.6 48.9 %all-gather.9.cloned.1.call-done = bf16[512,2048]{0,1:T(8,128)(2,1)} async-done(((bf16[512,128]{0,1:T(8,128)(2,1)}), bf16[512,2048]{0,1:T(8,128)(2,1)}) %all-gather.9.cloned.1.call-update) | async-done | bytes 2097168 | tf_op jit(solution)/shard_map/all_gather | solution.py:184
  296.5 3.0 fusion.36
  (195 shorter events, 59.2 us)
Async XLA Ops:
  6.5 289.9 %copy-start = (bf16[2048,256]{1,0:T(8,128)(2,1)S(1)}, bf16[2048,256]{1,0:T(8,128)(2,1)}, u32[]{:S(2)}) copy-start(bf16[2048,256]{1,0:T(8,128)(2,1)} %param.29) | copy-start | bytes 3145732
  6.6 48.9 %copy-start.6 = (f32[256]{0:T(256)S(1)}, f32[256]{0:T(256)}, u32[]{:S(2)}) copy-start(f32[256]{0:T(256)} %param.21) | copy-start | bytes 3076
  6.6 97.7 %all-gather.5.cloned.1.call-start = ((), (), s32[]{:S(2)}) async-start(), calls=%async_computation.2 | async-start | bytes 5013504 | tf_op jit(solution)/shard_map/all_gather | solution.py:27
  11.2 63.2 %all-to-all-start = ((f32[16,2,3,256]{3,1,2,0:T(2,128)}), f32[16,2,3,256]{3,1,2,0:T(2,128)S(1)}, u32[]{:S(2)}, u32[]{:S(2)}) async-start(f32[16,2,3,256]{3,1,2,0:T(2,128)} %broadcast_in_dim.16), calls=%async_computation | async-start | bytes 196608 | tf_op jit(solution)/shard_map/all_to_all | solution.py:15
  75.1 12.9 %all-to-all-start.1 = ((f32[16,2,2,256]{3,2,1,0:T(2,128)}), f32[16,2,2,256]{3,2,1,0:T(2,128)S(1)}, u32[]{:S(2)}, u32[]{:S(2)}) async-start(f32[16,2,2,256]{3,2,1,0:T(2,128)} %stack.2), calls=%async_computation.1 | async-start | bytes 131072 | tf_op jit(solution)/shard_map/all_to_all | solution.py:104
  79.5 108.2 %all-gather.7.cloned.1.call-start = ((), (), s32[]{:S(2)}) async-start(), calls=%async_computation.3 | async-start | bytes 4456448 | tf_op jit(solution)/shard_map/all_gather | solution.py:27
  107.3 3.4 %copy-start.2 = (bf16[4096,128]{1,0:T(8,128)(2,1)S(1)}, bf16[4096,128]{1,0:T(8,128)(2,1)}, u32[]{:S(2)}) copy-start(bf16[4096,128]{1,0:T(8,128)(2,1)} %param.24) | copy-start | bytes 3145732
  110.8 2.0 copy-start.1
  110.8 2.0 copy-start.3
  112.8 1.6 copy-start.7
  115.3 181.2 %all-gather.9.cloned.1.call-start = ((), (), s32[]{:S(2)}) async-start(), calls=%async_computation.4 | async-start | bytes 2228224 | tf_op jit(solution)/shard_map/all_gather | solution.py:184
  119.7 1.6 copy-start.4
  121.3 3.8 %copy-start.8 = (f32[64]{0:T(128)S(1)}, f32[64]{0:T(128)}, u32[]{:S(2)}) copy-start(f32[64]{0:T(128)} %param.25) | copy-start | bytes 772
  192.2 54.5 %copy-start.9 = (f32[128]{0:T(128)S(1)}, f32[128]{0:T(128)}, u32[]{:S(2)}) copy-start(f32[128]{0:T(128)} %param.28) | copy-start | bytes 1540
  192.2 104.2 %copy-start.5 = (bf16[512,256]{1,0:T(8,128)(2,1)S(1)}, bf16[512,256]{1,0:T(8,128)(2,1)}, u32[]{:S(2)}) copy-start(bf16[512,256]{1,0:T(8,128)(2,1)} %param.17) | copy-start | bytes 786436
Sparse Core Ops, SparseCore 0:
  9.4 94.7 all-gather.4
  115.4 72.1 all-gather.6
  247.7 48.7 all-gather.8
